TPU v7x, 32 devices: a whole 2x2x4 slice. The times are simulated.
32 devices in a mesh: sp: 16 (over z, y, core), tp: 2 (over x).
Axes of the slice: x: 2, y: 2, z: 4, core: 2. Of those that a mesh axis runs over, the one named last changes fastest.
Arguments:
- inputs: bfloat16 [2, 2048, 1024], P(None, 'sp'), may hold values from -6 to 6
- queries: bfloat16 [2, 2048, 4, 128], P(None, 'sp', 'tp'), may hold values from -6 to 6
- values: bfloat16 [2, 2048, 4, 256], P(None, 'sp', 'tp'), may hold values from -6 to 6
- out_grad: bfloat16 [2, 2048, 4, 256], P(None, 'sp', 'tp'), may hold values from -6 to 6
- key_weight: bfloat16 [1024, 4, 128], P(None, 'tp'), may hold values from -6 to 6
- decay_ahead: float32 [4], P('tp'), may hold values from -2.9 to 2.2
- decay_behind: float32 [4], P('tp'), may hold values from -2.9 to 2.2
Outputs:
- query_grad: bfloat16 [2, 2048, 4, 128], P(None, 'sp', 'tp')
- value_grad: bfloat16 [2, 2048, 4, 256], P(None, 'sp', 'tp')
- input_grad: bfloat16 [2, 2048, 1024], P('tp', 'sp')
- weight_grad: float32 [1024, 4, 128], P('sp', 'tp')
- decay_grad: float32 [2, 4], P(None, 'tp')
All inputs are finite; a program needn't handle non-finite values.
Results may differ from a plain program's by a relative error of at most 0.015.
Values may be sent and summed in bfloat16 or wider, within the bound.
A program may use at most 256 MiB of HBM per device.

v0:
```python
import math

import jax
import jax.numpy as jnp
from jax import lax
from jax.sharding import PartitionSpec as P

HIGHEST = lax.Precision.HIGHEST


def prefix(value, axis, join, neutral, backward):
    count, mine = lax.axis_size(axis), lax.axis_index(axis)
    pieces = jax.tree.map(lambda part: lax.all_gather(part, axis), value)
    if backward:
        pieces = jax.tree.map(lambda part: part[::-1], pieces)
        mine = count - 1 - mine
    subtotal = jax.tree.map(
        lambda part, zero: jnp.full_like(part, 0) + jnp.asarray(zero, part.dtype), value, neutral
    )

    def step(position, subtotal):
        longer = join(subtotal, jax.tree.map(lambda part: part[position], pieces))
        return jax.tree.map(lambda new, old: jnp.where(position < mine, new, old), longer, subtotal)

    return lax.fori_loop(0, count - 1, step, subtotal)


def own_rows(contribution, rows, axis):
    whole = contribution(jnp.int32(0), rows * lax.axis_size(axis))
    return lax.psum_scatter(whole, axis, scatter_dimension=0, tiled=True)


def summed_rows(product, rows, axis):
    everything = product(jnp.int32(0), lax.axis_size(axis) * rows)
    own = lax.psum_scatter(everything.astype(jnp.bfloat16), axis, scatter_dimension=0, tiled=True)
    return own.astype(jnp.float32)


def link_states(earlier, later):
    return (
        earlier[0] * later[0],
        later[0] * earlier[1] + later[1],
        earlier[2] * later[2],
        later[2] * earlier[3] + later[3],
    )


def shards(inputs, queries, values, out_grad, key_weight, decay_ahead, decay_behind):
    batch_seqs, length, in_width = inputs.shape
    devices = lax.axis_size("sp")
    my_index = lax.axis_index("sp").astype(jnp.float32)
    all_tokens = length * devices
    key_scale = 1.0 / math.sqrt(in_width * queries.shape[3] * all_tokens)
    rate_ahead = jax.nn.log_sigmoid(decay_ahead) / all_tokens
    rate_behind = jax.nn.log_sigmoid(decay_behind) / all_tokens
    key_raw = jnp.einsum(
        "bld,dhk->blhk", inputs, key_weight, preferred_element_type=jnp.float32
    ).astype(jnp.bfloat16)
    keys = key_raw.astype(jnp.float32) * key_scale
    query_wide = queries.astype(jnp.float32)
    value_wide = values.astype(jnp.float32)
    grad_wide = out_grad.astype(jnp.float32)
    offsets = jnp.arange(length, dtype=jnp.float32)
    distance = offsets[:, None] - offsets[None, :]
    mask_ahead = jnp.where(
        distance[None] >= 0, jnp.exp(distance[None] * rate_ahead[:, None, None]), 0.0
    )
    mask_behind = jnp.where(
        distance[None] <= 0, jnp.exp(-distance[None] * rate_behind[:, None, None]), 0.0
    )
    mask_both = (mask_ahead + mask_behind)[None]
    keep_ahead = jnp.exp((length - 1.0 - offsets)[:, None] * rate_ahead[None])[None, :, :, None]
    keep_behind = jnp.exp(offsets[:, None] * rate_behind[None])[None, :, :, None]
    reach_ahead = jnp.exp((offsets + 1.0)[:, None] * rate_ahead[None])[None, :, :, None]
    reach_behind = jnp.exp((length - offsets)[:, None] * rate_behind[None])[None, :, :, None]
    scores = (
        jnp.einsum("bthk,bshk->bhts", queries, key_raw, preferred_element_type=jnp.float32)
        * key_scale
    )
    grad_scores = jnp.einsum(
        "bthv,bshv->bhts", out_grad, values, preferred_element_type=jnp.float32
    )
    sums_ahead = jnp.einsum("bshk,bshv->bhkv", keys * keep_ahead, value_wide, precision=HIGHEST)
    sums_behind = jnp.einsum("bshk,bshv->bhkv", keys * keep_behind, value_wide, precision=HIGHEST)
    pulls_ahead = jnp.einsum(
        "bthk,bthv->bhkv", query_wide * reach_ahead, grad_wide, precision=HIGHEST
    )
    pulls_behind = jnp.einsum(
        "bthk,bthv->bhkv", query_wide * reach_behind, grad_wide, precision=HIGHEST
    )
    span_ahead = jnp.exp(length * rate_ahead).reshape(1, -1, 1, 1)
    span_behind = jnp.exp(length * rate_behind).reshape(1, -1, 1, 1)
    unit_span = jnp.ones_like(span_ahead)
    zero_state = jnp.zeros_like(sums_ahead)
    upward = prefix(
        (span_ahead, sums_ahead, span_behind, pulls_behind),
        "sp",
        link_states,
        (unit_span, zero_state, unit_span, zero_state),
        False,
    )
    downward = prefix(
        (span_behind, sums_behind, span_ahead, pulls_ahead),
        "sp",
        link_states,
        (unit_span, zero_state, unit_span, zero_state),
        True,
    )
    state_ahead, pull_behind = (upward[1], upward[3])
    state_behind, pull_ahead = (downward[1], downward[3])
    out_ahead = jnp.einsum(
        "bhts,bshv->bthv", scores * mask_ahead[None], value_wide, precision=HIGHEST
    )
    out_ahead = out_ahead + jnp.einsum(
        "bthk,bhkv->bthv", query_wide * reach_ahead, state_ahead, precision=HIGHEST
    )
    out_behind = jnp.einsum(
        "bhts,bshv->bthv", scores * mask_behind[None], value_wide, precision=HIGHEST
    )
    out_behind = out_behind + jnp.einsum(
        "bthk,bhkv->bthv", query_wide * reach_behind, state_behind, precision=HIGHEST
    )
    grad_q = jnp.einsum("bhts,bshk->bthk", grad_scores * mask_both, keys, precision=HIGHEST)
    grad_q = grad_q + reach_ahead * jnp.einsum(
        "bthv,bhkv->bthk", grad_wide, state_ahead, precision=HIGHEST
    )
    grad_q = grad_q + reach_behind * jnp.einsum(
        "bthv,bhkv->bthk", grad_wide, state_behind, precision=HIGHEST
    )
    grad_k_ahead = jnp.einsum(
        "bhts,bthk->bshk", grad_scores * mask_ahead[None], query_wide, precision=HIGHEST
    )
    grad_k_ahead = grad_k_ahead + keep_ahead * jnp.einsum(
        "bshv,bhkv->bshk", value_wide, pull_ahead, precision=HIGHEST
    )
    grad_k_behind = jnp.einsum(
        "bhts,bthk->bshk", grad_scores * mask_behind[None], query_wide, precision=HIGHEST
    )
    grad_k_behind = grad_k_behind + keep_behind * jnp.einsum(
        "bshv,bhkv->bshk", value_wide, pull_behind, precision=HIGHEST
    )
    grad_v = jnp.einsum("bhts,bthv->bshv", scores * mask_both, grad_wide, precision=HIGHEST)
    grad_v = grad_v + keep_ahead * jnp.einsum(
        "bshk,bhkv->bshv", keys, pull_ahead, precision=HIGHEST
    )
    grad_v = grad_v + keep_behind * jnp.einsum(
        "bshk,bhkv->bshv", keys, pull_behind, precision=HIGHEST
    )
    positions = (my_index * length + offsets)[None, :, None]
    out_dot_ahead = jnp.sum(positions * jnp.sum(out_ahead * grad_wide, axis=3), axis=(0, 1))
    key_dot_ahead = jnp.sum(positions * jnp.sum(keys * grad_k_ahead, axis=3), axis=(0, 1))
    out_dot_behind = jnp.sum(positions * jnp.sum(out_behind * grad_wide, axis=3), axis=(0, 1))
    key_dot_behind = jnp.sum(positions * jnp.sum(keys * grad_k_behind, axis=3), axis=(0, 1))
    local_sums = jnp.stack([out_dot_ahead - key_dot_ahead, key_dot_behind - out_dot_behind])
    rate_sums = lax.psum(local_sums, "sp")
    slopes = jnp.stack([jax.nn.sigmoid(-decay_ahead), jax.nn.sigmoid(-decay_behind)]) / all_tokens
    decay_grad = rate_sums * slopes
    key_grad_raw = ((grad_k_ahead + grad_k_behind) * key_scale).astype(jnp.bfloat16)

    def weight_rows(start, row_count):
        piece = lax.dynamic_slice_in_dim(inputs, start, row_count, 2)
        return jnp.einsum("bld,blhk->dhk", piece, key_grad_raw, preferred_element_type=jnp.float32)

    weight_grad = own_rows(weight_rows, in_width // devices, "sp")

    def input_rows(start, row_count):
        piece = lax.dynamic_slice_in_dim(key_grad_raw, start, row_count, 0)
        return jnp.einsum("blhk,dhk->bld", piece, key_weight, preferred_element_type=jnp.float32)

    input_grad = summed_rows(input_rows, batch_seqs // lax.axis_size("tp"), "tp").astype(
        jnp.bfloat16
    )
    return (
        grad_q.astype(jnp.bfloat16),
        grad_v.astype(jnp.bfloat16),
        input_grad,
        weight_grad,
        decay_grad,
    )


def solution(mesh):
    in_specs = (
        P(None, "sp", None),
        P(None, "sp", "tp", None),
        P(None, "sp", "tp", None),
        P(None, "sp", "tp", None),
        P(None, "tp", None),
        P("tp"),
        P("tp"),
    )
    out_specs = (
        P(None, "sp", "tp", None),
        P(None, "sp", "tp", None),
        P("tp", "sp", None),
        P("sp", "tp", None),
        P(None, "tp"),
    )
    return jax.shard_map(shards, mesh=mesh, in_specs=in_specs, out_specs=out_specs, check_vma=False)
```

profile of v0, /device:TPU:0, one launch (start us, length us, event | category | flops | bytes accessed | tf_op | source)
XLA Modules:
  0.0 462.0 jit_solution(7390019577858132643)
XLA Ops:
  7.3 1.4 copy.106
  8.7 1.3 broadcast_multiply_fusion.3
  10.9 2.1 fusion.41
  14.8 2.1 fusion.37
  17.1 2.1 fusion.40
  19.3 2.1 fusion.36
  21.5 1.3 fusion.92
  23.7 35.5 %all-reduce.3 = (f32[32]{0:T(128)S(1)}, f32[32]{0:T(128)S(1)}) all-reduce(f32[32]{0:T(128)S(1)} %exponential_dynamic-update-slice_fusion, f32[32]{0:T(128)S(1)} %exponential_dynamic-update-slice_fusion.1), channel_id=4, replica_groups=mesh['sp'=16,'tp'=2] {'sp'}, use_global_device_ids=true, to_apply=%add.1 | all-reduce | flops 64 | bytes 512
  60.7 1.6 broadcast_multiply_fusion
  62.3 1.7 copy.122
  63.9 1.7 copy.144
  69.4 21.4 %all-gather.15.cloned.1.call-done = f32[32,2,128,256]{3,2,1,0:T(8,128)} async-done(((f32[2,2,128,256]{3,2,1,0:T(8,128)}), f32[32,2,128,256]{3,2,1,0:T(8,128)}) %all-gather.15.cloned.1.call-update) | async-done | bytes 8388624 | tf_op jit(solution)/shard_map/all_gather | solution.py:13
  90.8 7.6 %rev.13 = f32[16,2,2,128,256]{4,3,2,1,0:T(8,128)} reverse(f32[16,2,2,128,256]{4,3,2,1,0:T(8,128)} %bitcast.160), dimensions={0} | reverse | bytes 16777216 | tf_op jit(solution)/shard_map/rev | solution.py:15
  98.4 67.4 %all-gather.17.cloned.1.call-done = f32[32,2,128,256]{3,2,1,0:T(8,128)} async-done(((f32[2,2,128,256]{3,2,1,0:T(8,128)}), f32[32,2,128,256]{3,2,1,0:T(8,128)}) %all-gather.17.cloned.1.call-update) | async-done | bytes 8388624 | tf_op jit(solution)/shard_map/all_gather | solution.py:13
  165.8 7.6 %rev.15 = f32[16,2,2,128,256]{4,3,2,1,0:T(8,128)} reverse(f32[16,2,2,128,256]{4,3,2,1,0:T(8,128)} %bitcast.161), dimensions={0} | reverse | bytes 16777216 | tf_op jit(solution)/shard_map/rev | solution.py:15
  173.4 41.8 %while.33 = (s32[]{:T(128)}, f32[2,2,128,256]{3,2,1,0:T(8,128)S(1)}, f32[2,2,128,256]{3,2,1,0:T(8,128)S(1)}, s32[]{:T(128)}, f32[16,1,2,1,1]{2,4,3,1,0:T(1,128)}...) while((s32[]{:T(128)}, ...), condition=%wide.region_3.4_spmd.clone, body=%wide.region_2.3_spmd.clone.sunk | while | flops 1048580 | bytes 3145917 | solution.py:25
  174.7 1.5 fusion.118
  177.4 1.5 fusion.118
  180.2 1.5 fusion.118
  183.0 1.5 fusion.118
  185.8 1.5 fusion.118
  188.6 1.5 fusion.118
  191.3 1.5 fusion.118
  194.2 1.5 fusion.118
  197.0 1.5 fusion.118
  199.8 1.5 fusion.118
  202.5 1.5 fusion.118
  205.4 1.5 fusion.118
  208.1 1.5 fusion.118
  210.9 1.5 fusion.118
  213.8 1.5 fusion.118
  216.4 1.4 convolution_bitcast_fusion.2
  217.8 23.0 %all-gather.11.cloned.1.call-done = f32[32,2,128,256]{3,2,1,0:T(8,128)} async-done(((f32[2,2,128,256]{3,2,1,0:T(8,128)}), f32[32,2,128,256]{3,2,1,0:T(8,128)}) %all-gather.11.cloned.1.call-update) | async-done | bytes 8388624 | tf_op jit(solution)/shard_map/all_gather | solution.py:13
  240.8 74.8 %all-gather.13.cloned.1.call-done = f32[32,2,128,256]{3,2,1,0:T(8,128)} async-done(((f32[2,2,128,256]{3,2,1,0:T(8,128)}), f32[32,2,128,256]{3,2,1,0:T(8,128)}) %all-gather.13.cloned.1.call-update) | async-done | bytes 8388624 | tf_op jit(solution)/shard_map/all_gather | solution.py:13
  315.7 23.2 %while.32 = (s32[]{:T(128)}, f32[2,2,128,256]{3,2,1,0:T(8,128)S(1)}, f32[2,2,128,256]{3,2,1,0:T(8,128)S(1)}, s32[]{:T(128)}, f32[16,1,2,1,1]{2,4,3,1,0:T(1,128)S...) while((s32[]{:T(128)}, ...), condition=%wide.region_1.2_spmd.clone, body=%wide.region_0.1_spmd.clone.sunk | while | flops 1048580 | bytes 3145917 | solution.py:25
  315.7 1.5 fusion.115
  317.3 1.5 fusion.115
  318.8 1.5 fusion.115
  320.3 1.5 fusion.115
  321.9 1.5 fusion.115
  323.4 1.5 fusion.115
  325.0 1.5 fusion.115
  326.5 1.5 fusion.115
  328.1 1.5 fusion.115
  329.6 1.5 fusion.115
  331.2 1.5 fusion.115
  332.7 1.5 fusion.115
  334.2 1.5 fusion.115
  335.8 1.5 fusion.115
  337.3 1.5 fusion.115
  338.9 1.1 fusion.20
  341.4 1.8 fusion.38
  343.2 1.3 convolution_bitcast_fusion
  344.5 2.2 copy.136
  347.5 1.6 fusion.18
  349.1 1.4 fusion.19
  351.8 31.2 %psum.7 = f32[2,2]{1,0:T(2,128)S(1)} all-reduce(f32[2,2]{1,0:T(2,128)S(1)} %pad_maximum_fusion), channel_id=1, replica_groups=mesh['sp'=16,'tp'=2] {'sp'}, use_global_device_ids=true, to_apply=%region_14.15 | all-reduce | flops 4 | bytes 32 | tf_op jit(solution)/shard_map/psum | solution.py:155
  383.0 1.7 fusion.28
  385.4 2.2 fusion.8
  389.0 1.3 fusion.17
  391.2 1.3 fusion.83
  392.5 46.4 %all-reduce.6.cloned.1.call-done = f32[1024,2,128]{2,1,0:T(2,128)} async-done(((f32[1024,2,128]{2,1,0:T(2,128)}), f32[1024,2,128]{2,1,0:T(2,128)}) %all-reduce.6.cloned.1.call-update) | async-done | bytes 1048592
  438.8 1.5 constant_dynamic-slice_fusion.4
  440.3 14.8 %reduce-scatter.2.cloned.1.call-done = bf16[1,128,1024]{2,1,0:T(8,128)(2,1)} async-done(((bf16[2,128,1024]{2,1,0:T(8,128)(2,1)}), bf16[1,128,1024]{2,1,0:T(8,128)(2,1)}) %reduce-scatter.2.cloned.1.call-update) | async-done | bytes 262160 | tf_op jit(solution)/shard_map/reduce_scatter | solution.py:35
  (137 shorter events, 34.8 us)
Async XLA Ops:
  7.2 2.8 copy-start
  7.2 61.3 %copy-start.2 = (bf16[2,128,2,256]{3,2,1,0:T(2,128)(2,1)S(1)}, bf16[2,128,2,256]{3,2,1,0:T(2,128)(2,1)}, u32[]{:S(2)}) copy-start(bf16[2,128,2,256]{3,2,1,0:T(2,128)(2,1)} %param.13) | copy-start | bytes 786436
  7.2 61.3 %copy-start.1 = (bf16[2,128,2,256]{3,2,1,0:T(2,128)(2,1)S(1)}, bf16[2,128,2,256]{3,2,1,0:T(2,128)(2,1)}, u32[]{:S(2)}) copy-start(bf16[2,128,2,256]{3,2,1,0:T(2,128)(2,1)} %param.14) | copy-start | bytes 786436
  7.2 83.6 %all-gather.15.cloned.1.call-start = ((), (), s32[]{:S(2)}) async-start(), calls=%async_computation.4 | async-start | bytes 8912896 | tf_op jit(solution)/shard_map/all_gather | solution.py:13
  9.9 11.6 %copy-start.12 = (f32[2]{0:T(128)}, f32[2]{0:T(128)S(1)}, u32[]{:S(2)}) copy-start(f32[2]{0:T(128)S(1)} %get-tuple-element.478) | copy-start | bytes 28
  9.9 11.6 %copy-start.13 = (f32[2]{0:T(128)}, f32[2]{0:T(128)S(1)}, u32[]{:S(2)}) copy-start(f32[2]{0:T(128)S(1)} %get-tuple-element.450) | copy-start | bytes 28
  10.9 10.5 %copy-start.8 = (f32[128,2]{0,1:T(2,128)}, f32[128,2]{0,1:T(2,128)S(1)}, u32[]{:S(2)}) copy-start(f32[128,2]{0,1:T(2,128)S(1)} %get-tuple-element.470) | copy-start | bytes 3076
  13.1 152.7 %all-gather.17.cloned.1.call-start = ((), (), s32[]{:S(2)}) async-start(), calls=%async_computation.5 | async-start | bytes 8912896 | tf_op jit(solution)/shard_map/all_gather | solution.py:13
  14.8 6.6 %copy-start.6 = (f32[128,2]{0,1:T(2,128)}, f32[128,2]{0,1:T(2,128)S(1)}, u32[]{:S(2)}) copy-start(f32[128,2]{0,1:T(2,128)S(1)} %get-tuple-element.467) | copy-start | bytes 3076
  17.0 223.8 %all-gather.11.cloned.1.call-start = ((), (), s32[]{:S(2)}) async-start(), calls=%async_computation.2 | async-start | bytes 8912896 | tf_op jit(solution)/shard_map/all_gather | solution.py:13
  19.2 296.4 %all-gather.13.cloned.1.call-start = ((), (), s32[]{:S(2)}) async-start(), calls=%async_computation.3 | async-start | bytes 8912896 | tf_op jit(solution)/shard_map/all_gather | solution.py:13
  21.4 417.5 %all-reduce.6.cloned.1.call-start = ((), (), s32[]{:S(2)}) async-start(), calls=%async_computation.6 | async-start | bytes 2097152
  173.4 41.8 %copy-start.9 = (f32[128,2]{0,1:T(2,128)S(1)}, f32[128,2]{0,1:T(2,128)}, u32[]{:S(2)}) copy-start(f32[128,2]{0,1:T(2,128)} %copy-done.8) | copy-start | bytes 3076
  315.6 25.4 %copy-start.3 = (f32[2,2,128,128]{3,2,1,0:T(8,128)S(1)}, f32[2,2,128,128]{3,2,1,0:T(8,128)}, u32[]{:S(2)}) copy-start(f32[2,2,128,128]{3,2,1,0:T(8,128)} %fusion.72) | copy-start | bytes 786436
  315.7 25.4 %copy-start.5 = (f32[2,128,128]{2,1,0:T(8,128)S(1)}, f32[2,128,128]{2,1,0:T(8,128)}, u32[]{:S(2)}) copy-start(f32[2,128,128]{2,1,0:T(8,128)} %get-tuple-element.459) | copy-start | bytes 393220
  338.8 8.0 %copy-start.7 = (f32[128,2]{0,1:T(2,128)S(1)}, f32[128,2]{0,1:T(2,128)}, u32[]{:S(2)}) copy-start(f32[128,2]{0,1:T(2,128)} %copy-done.6) | copy-start | bytes 3076
  338.8 8.6 %copy-start.4 = (f32[2,2,128,128]{2,3,1,0:T(8,128)S(1)}, f32[2,2,128,128]{2,3,1,0:T(8,128)}, u32[]{:S(2)}) copy-start(f32[2,2,128,128]{2,3,1,0:T(8,128)} %convolution_bitcast_fusion.16) | copy-start | bytes 786436
  340.0 47.7 %copy-start.10 = (f32[128,2]{0,1:T(2,128)S(1)}, f32[128,2]{0,1:T(2,128)}, u32[]{:S(2)}) copy-start(f32[128,2]{0,1:T(2,128)} %get-tuple-element.468) | copy-start | bytes 3076
  341.0 47.3 %copy-start.11 = (f32[128,2]{0,1:T(2,128)S(1)}, f32[128,2]{0,1:T(2,128)}, u32[]{:S(2)}) copy-start(f32[128,2]{0,1:T(2,128)} %get-tuple-element.461) | copy-start | bytes 3076
  346.7 108.4 %reduce-scatter.2.cloned.1.call-start = ((), (), s32[]{:S(2)}) async-start(), calls=%async_computation.1 | async-start | bytes 786432 | tf_op jit(solution)/shard_map/reduce_scatter | solution.py:35
Sparse Core Ops, SparseCore 0:
  13.2 77.5 all-gather.14
  93.0 72.7 all-gather.16
  168.0 72.7 all-gather.10
  242.8 72.7 all-gather.12
  346.9 91.9 all-reduce.5
  441.5 13.5 reduce-scatter.1
where the time goes:
time: 464 us; the launch traced here: 462 us
  waiting for transfers between devices  248 us (53%)
  blocking collectives  66.7 us (14%)
  other arithmetic  51.5 us (11%)
  local copies, waits for them, and re-layouts  49.5 us (11%)
  matrix products  29.3 us (6%)
  between operations  15.8 us (3%)
    all_gather x4, waiting for transfers between devices, prefix(): pieces = jax.tree.map(lambda part: lax.all_gather(part, axis), value)  187 us
    unnamed x7, waiting for transfers between devices  46.5 us
    select_n x30, other arithmetic, step(): jnp.where(position < mine, new, old)  44.4 us
    unnamed x1, blocking collectives  35.5 us
    psum x1, blocking collectives, shards(): rate_sums = lax.psum(local_sums, 'sp')  31.2 us
    rev x4, local copies, waits for them, and re-layouts, prefix(): pieces = jax.tree.map(lambda part: part[::-1], pieces)  16.4 us
    reduce_scatter x1, waiting for transfers between devices, summed_rows(): lax.psum_scatter(everything.astype(jnp.bfloat16), axis, scatter_dimension...  14.8 us
    mul x30, local copies, waits for them, and re-layouts, link_states(): later[0] * earlier[1] + later[1]  9.93 us
  transfers between devices with their start and end apart: 6, of which 6 were waited for; matrix products, arithmetic and copies ran while one was open for 20% of the time, Pallas kernels for 0%

commit v1 on v0

v1 whole, which is shorter than its diff:
```python
import functools
import math

import jax
import jax.numpy as jnp
from jax import lax
from jax.experimental import pallas as pl
from jax.experimental.pallas import tpu as pltpu
from jax.sharding import PartitionSpec as P

F32 = jnp.float32
BF16 = jnp.bfloat16
NN = (((1,), (0,)), ((), ()))
NT = (((1,), (1,)), ((), ()))
TN = (((0,), (0,)), ((), ()))


def mm(a, b, dims):
    return lax.dot_general(a, b, dims, preferred_element_type=F32)


def kernel(
    cfg,
    rates, pack, x, w,
    gqv_out, ig_out, wg_out, dec_out,
    tok, ktok, kown, local, arrive, leave,
    kgs, kgr, gqs, gqr, dbuf, dpair, dsum, dland,
    wb, wpair, wsum, wland, isend, iland,
    tok_s, tok_r, k_s, k_r, ch_s, ch_r, kg_s, kg_r, gq_s, gq_r,
    tp_s, tp_r, pr_s, pr_r, w_s, w_r, d_s, d_r,
):
    n, tp, seqs, heads, length, dk, dv, scale = cfg
    pairs = seqs * heads
    groups = n // pairs
    half = n // 2
    chunk = pairs * length
    me = lax.axis_index("sp")
    my_tp = lax.axis_index("tp")
    group = me // pairs
    member = me % pairs
    base = group * pairs
    parity = me % 2
    mine = me // 2
    partner = me + 1 - 2 * parity
    head = member % heads

    def remote(src, dst, send, recv, device):
        return pltpu.make_async_remote_copy(
            src_ref=src, dst_ref=dst, send_sem=send, recv_sem=recv,
            device_id=device, device_id_type=pl.DeviceIdType.MESH,
        )

    barrier = pltpu.get_barrier_semaphore()
    greeted = 0
    for o in range(1, half):
        pl.semaphore_signal(
            barrier, inc=1, device_id={"sp": 2 * ((mine + o) % half) + parity},
            device_id_type=pl.DeviceIdType.MESH)
        greeted += 1
    for o in range(1, pairs, 2):
        pl.semaphore_signal(
            barrier, inc=1, device_id={"sp": base + (member + o) % pairs},
            device_id_type=pl.DeviceIdType.MESH)
        greeted += 1
    for o in range(1, tp):
        pl.semaphore_signal(
            barrier, inc=1, device_id={"tp": (my_tp + o) % tp},
            device_id_type=pl.DeviceIdType.MESH)
        greeted += 1
    pl.semaphore_wait(barrier, greeted)

    tok_copies, k_copies = [], []
    for o in range(1, pairs):
        to = (member + o) % pairs
        copy = remote(pack.at[to], tok.at[member], tok_s.at[o], tok_r.at[o], {"sp": base + to})
        copy.start()
        tok_copies.append(copy)
    key_raw = mm(x[...], w[...], NN).astype(BF16)
    for b in range(seqs):
        for h in range(heads):
            kown[b * heads + h] = key_raw[b * length:(b + 1) * length, h * dk:(h + 1) * dk]
    for o in range(1, pairs):
        to = (member + o) % pairs
        copy = remote(kown.at[to], ktok.at[member], k_s.at[o], k_r.at[o], {"sp": base + to})
        copy.start()
        k_copies.append(copy)
    tok[member] = pack[member]
    ktok[member] = kown[member]

    rate_a = rates[0, head]
    rate_b = rates[1, head]
    off = lax.broadcasted_iota(jnp.int32, (chunk, 1), 0).astype(F32)
    keep_a = jnp.exp((chunk - 1.0 - off) * rate_a)
    keep_b = jnp.exp(off * rate_b)
    reach_a = jnp.exp((off + 1.0) * rate_a)
    reach_b = jnp.exp((chunk - off) * rate_b)
    one = jnp.full((1, dv), float(chunk), F32)
    spans = (jnp.exp(one * rate_a), jnp.exp(one * rate_b))

    for copy in tok_copies:
        copy.wait_recv()
    q = tok[:, :, :dk].reshape(chunk, dk)
    v = tok[:, :, dk:dk + dv].reshape(chunk, dv)
    do = tok[:, :, dk + dv:].reshape(chunk, dv)
    qf = q.astype(F32)
    local[0, 1] = mm((qf * reach_b).astype(BF16), do, TN)
    local[1, 0] = mm((qf * reach_a).astype(BF16), do, TN)
    for copy in k_copies:
        copy.wait_recv()
    k = ktok[...].reshape(chunk, dk)
    kf = k.astype(F32)
    local[0, 0] = mm((kf * keep_a).astype(BF16), v, TN)
    local[1, 1] = mm((kf * keep_b).astype(BF16), v, TN)

    low = group < (groups + 1) // 2

    def chain(j):
        way = jnp.where(low, j, 1 - j)
        has_in = jnp.where(way == 0, group > 0, group < groups - 1)
        has_out = jnp.where(way == 0, group < groups - 1, group > 0)
        nxt = jnp.clip(group + 1 - 2 * way, 0, groups - 1) * pairs + member
        for kind in range(2):
            copy = remote(leave.at[way, kind], arrive.at[way, kind], ch_s.at[way, kind],
                          ch_r.at[way, kind], {"sp": nxt})

            @pl.when(has_in)
            def _():
                copy.wait_recv()

            @pl.when(jnp.logical_not(has_in))
            def _():
                arrive[way, kind] = jnp.zeros(arrive.shape[2:], BF16)

            @pl.when(has_out)
            def _():
                leave[way, kind] = (
                    spans[kind] * arrive[way, kind].astype(F32) + local[way, kind]
                ).astype(BF16)
                copy.start()

    def chain_end(j):
        way = jnp.where(low, j, 1 - j)
        has_out = jnp.where(way == 0, group < groups - 1, group > 0)
        nxt = jnp.clip(group + 1 - 2 * way, 0, groups - 1) * pairs + member
        for kind in range(2):
            copy = remote(leave.at[way, kind], arrive.at[way, kind], ch_s.at[way, kind],
                          ch_r.at[way, kind], {"sp": nxt})

            @pl.when(has_out)
            def _():
                copy.wait_send()

    chain(0)
    scores = mm(q, k, NT) * scale
    grads = mm(do, v, NT)
    dist = (lax.broadcasted_iota(jnp.int32, (chunk, chunk), 0)
            - lax.broadcasted_iota(jnp.int32, (chunk, chunk), 1)).astype(F32)
    gap = jnp.abs(dist)
    decay = jnp.exp(gap * jnp.where(dist >= 0, rate_a, rate_b))
    mask = jnp.where(dist == 0, 2.0, decay)
    gm = grads * mask
    weighted = gm * scores * gap
    in_a = jnp.sum(jnp.where(dist > 0, weighted, 0.0))
    in_b = jnp.sum(jnp.where(dist < 0, weighted, 0.0))
    gm = gm.astype(BF16)
    sm = (scores * mask).astype(BF16)
    grad_q = mm(gm, k, NN)
    grad_k = mm(gm, q, TN)
    grad_v = mm(sm, do, TN)
    chain(1)

    ka = keep_a * mm(v, arrive[1, 0], NT)
    kb = keep_b * mm(v, arrive[0, 1], NT)
    kgs[...] = ((grad_k + ka + kb) * scale).astype(BF16).reshape(pairs, length, dk)
    kg_copies = []
    for o in range(1, pairs):
        to = (member + o) % pairs
        copy = remote(kgs.at[to], kgr.at[member], kg_s.at[o], kg_r.at[o], {"sp": base + to})
        copy.start()
        kg_copies.append(copy)
    kgr[member] = kgs[member]
    qa = reach_a * mm(do, arrive[0, 0], NT)
    qb = reach_b * mm(do, arrive[1, 1], NT)
    gqs[:, :, :dk] = ((grad_q + qa + qb) * scale).astype(BF16).reshape(pairs, length, dk)
    far_v = keep_a * mm(k, arrive[1, 0], NN) + keep_b * mm(k, arrive[0, 1], NN)
    gqs[:, :, dk:] = (grad_v + far_v * scale).astype(BF16).reshape(pairs, length, dv)
    gq_copies = []
    for o in range(1, pairs):
        to = (member + o) % pairs
        copy = remote(gqs.at[to], gqr.at[member], gq_s.at[o], gq_r.at[o], {"sp": base + to})
        copy.start()
        gq_copies.append(copy)
    gqr[member] = gqs[member]
    pos = off + ((group * chunk).astype(F32) - 0.5 * (chunk * groups))
    sum_a = in_a + scale * jnp.sum(pos * (qf * qa - kf * ka))
    sum_b = in_b + scale * jnp.sum(pos * (kf * kb - qf * qb))
    row = lax.broadcasted_iota(jnp.int32, dbuf.shape, 0)
    lane = lax.broadcasted_iota(jnp.int32, dbuf.shape, 1)
    dbuf[...] = jnp.where(lane == head, jnp.where(row == 0, sum_a, jnp.where(row == 1, sum_b, 0.0)), 0.0)
    d_pair = remote(dbuf, dpair, pr_s.at[1], pr_r.at[1], {"sp": partner})
    d_pair.start()

    for copy in kg_copies:
        copy.wait_recv()
    own_seqs = seqs // tp
    tp_copies = []

    def seq_rows(b):
        return jnp.concatenate([kgr[b * heads + h] for h in range(heads)], axis=1)

    for o in range(1, tp):
        to = (my_tp + o) % tp
        for s in range(own_seqs):
            isend[o - 1, s * length:(s + 1) * length] = mm(
                seq_rows(to * own_seqs + s), w[...], NT).astype(BF16)
        copy = remote(isend.at[o - 1], iland.at[o - 1], tp_s.at[o - 1], tp_r.at[o - 1], {"tp": to})
        copy.start()
        tp_copies.append(copy)
    kg_all = jnp.concatenate([seq_rows(b) for b in range(seqs)], axis=0)
    wp = mm(x[...], kg_all, TN).astype(BF16).reshape(half, 2, -1, heads * dk)
    wb[0] = wp[:, 0]
    wb[1] = wp[:, 1]
    w_pair = remote(wb.at[1 - parity], wpair, pr_s.at[0], pr_r.at[0], {"sp": partner})
    w_pair.start()
    d_pair.wait_recv()
    dsum[...] = dbuf[...] + dpair[...]
    w_copies, d_copies = [], []
    for o in range(1, half):
        to = 2 * ((mine + o) % half) + parity
        copy = remote(dsum, dland.at[o - 1], d_s.at[o - 1], d_r.at[o - 1], {"sp": to})
        copy.start()
        d_copies.append(copy)
    own_ig = [mm(seq_rows(my_tp * own_seqs + s), w[...], NT) for s in range(own_seqs)]
    w_pair.wait_recv()
    wsum[...] = (wb[parity].astype(F32) + wpair[...].astype(F32)).astype(BF16)
    for o in range(1, half):
        j = (mine + o) % half
        copy = remote(wsum.at[j], wland.at[o - 1], w_s.at[o - 1], w_r.at[o - 1],
                      {"sp": 2 * j + parity})
        copy.start()
        w_copies.append(copy)
    for copy in gq_copies:
        copy.wait_recv()
    gqv_out[...] = gqr[...]
    for copy in tp_copies:
        copy.wait_recv()
    for s in range(own_seqs):
        total = own_ig[s]
        for o in range(tp - 1):
            total = total + iland[o, s * length:(s + 1) * length].astype(F32)
        ig_out[s * length:(s + 1) * length] = total.astype(BF16)
    total = dsum[...]
    for o, copy in enumerate(d_copies):
        copy.wait_recv()
        total = total + dland[o]
    dec_out[...] = total
    total = wsum[mine].astype(F32)
    for o, copy in enumerate(w_copies):
        copy.wait_recv()
        total = total + wland[o].astype(F32)
    wg_out[...] = total
    chain_end(0)
    chain_end(1)
    for copy in (tok_copies + k_copies + kg_copies + gq_copies + tp_copies + w_copies + d_copies
                 + [d_pair, w_pair]):
        copy.wait_send()


def shards(n, tp, inputs, queries, values, out_grad, key_weight, decay_ahead, decay_behind):
    seqs, length, width = inputs.shape
    heads, dk, dv = queries.shape[2], queries.shape[3], values.shape[3]
    pairs = seqs * heads
    all_tokens = length * n
    scale = 1.0 / math.sqrt(width * dk * all_tokens)
    decays = jnp.stack([decay_ahead, decay_behind])
    rates = jax.nn.log_sigmoid(decays) / all_tokens
    pack = jnp.concatenate([queries, values, out_grad], axis=3)
    pack = pack.transpose(0, 2, 1, 3).reshape(pairs, length, dk + 2 * dv)
    x = inputs.reshape(seqs * length, width)
    w = key_weight.reshape(width, heads * dk)
    half, rows, own = n // 2, width // n, seqs // tp
    vm = pl.BlockSpec(memory_space=pltpu.VMEM)
    dma = pltpu.SemaphoreType.DMA
    gqv, ig, wg, dec = pl.pallas_call(
        functools.partial(kernel, (n, tp, seqs, heads, length, dk, dv, scale)),
        out_shape=(
            jax.ShapeDtypeStruct((pairs, length, dk + dv), BF16),
            jax.ShapeDtypeStruct((own * length, width), BF16),
            jax.ShapeDtypeStruct((rows, heads * dk), F32),
            jax.ShapeDtypeStruct((8, 128), F32),
        ),
        in_specs=[pl.BlockSpec(memory_space=pltpu.SMEM), vm, vm, vm],
        out_specs=(vm, vm, vm, vm),
        scratch_shapes=[
            pltpu.VMEM((pairs, length, dk + 2 * dv), BF16),
            pltpu.VMEM((pairs, length, dk), BF16),
            pltpu.VMEM((pairs, length, dk), BF16),
            pltpu.VMEM((2, 2, dk, dv), F32),
            pltpu.VMEM((2, 2, dk, dv), BF16),
            pltpu.VMEM((2, 2, dk, dv), BF16),
            pltpu.VMEM((pairs, length, dk), BF16),
            pltpu.VMEM((pairs, length, dk), BF16),
            pltpu.VMEM((pairs, length, dk + dv), BF16),
            pltpu.VMEM((pairs, length, dk + dv), BF16),
            pltpu.VMEM((8, 128), F32),
            pltpu.VMEM((8, 128), F32),
            pltpu.VMEM((8, 128), F32),
            pltpu.VMEM((half - 1, 8, 128), F32),
            pltpu.VMEM((2, half, rows, heads * dk), BF16),
            pltpu.VMEM((half, rows, heads * dk), BF16),
            pltpu.VMEM((half, rows, heads * dk), BF16),
            pltpu.VMEM((half - 1, rows, heads * dk), BF16),
            pltpu.VMEM((tp - 1, own * length, width), BF16),
            pltpu.VMEM((tp - 1, own * length, width), BF16),
            dma((pairs,)), dma((pairs,)), dma((pairs,)), dma((pairs,)),
            dma((2, 2)), dma((2, 2)),
            dma((pairs,)), dma((pairs,)), dma((pairs,)), dma((pairs,)),
            dma((tp - 1,)), dma((tp - 1,)), dma((2,)), dma((2,)),
            dma((half - 1,)), dma((half - 1,)), dma((half - 1,)), dma((half - 1,)),
        ],
        compiler_params=pltpu.CompilerParams(
            collective_id=0, has_side_effects=True, vmem_limit_bytes=50 * 1024 * 1024
        ),
    )(rates, pack, x, w)
    gqv = gqv.reshape(seqs, heads, length, dk + dv).transpose(0, 2, 1, 3)
    slopes = jax.nn.sigmoid(-decays) / all_tokens
    return (
        gqv[..., :dk],
        gqv[..., dk:],
        ig.reshape(own, length, width),
        wg.reshape(rows, heads, dk),
        dec[:2, :heads] * slopes,
    )


def solution(mesh):
    in_specs = (
        P(None, "sp", None),
        P(None, "sp", "tp", None),
        P(None, "sp", "tp", None),
        P(None, "sp", "tp", None),
        P(None, "tp", None),
        P("tp"),
        P("tp"),
    )
    out_specs = (
        P(None, "sp", "tp", None),
        P(None, "sp", "tp", None),
        P("tp", "sp", None),
        P("sp", "tp", None),
        P(None, "tp"),
    )
    body = functools.partial(shards, mesh.shape["sp"], mesh.shape["tp"])
    return jax.shard_map(body, mesh=mesh, in_specs=in_specs, out_specs=out_specs, check_vma=False)
```

time: 464 us -> 50.1 us (0.11)
  waiting for transfers between devices: 248 us -> 0 us
  blocking collectives: 66.7 us -> 0 us
  other arithmetic: 51.5 us -> 1.9 us
  local copies, waits for them, and re-layouts: 49.5 us -> 5.82 us
  Pallas kernels: 0 us -> 41.4 us
  matrix products: 29.3 us -> 0 us
  between operations: 15.8 us -> 0.74 us
    all_gather x4 -> x0, waiting for transfers between devices: 187 us -> none  [prefix(): pieces = jax.tree.map(lambda part: lax.all_gather(part, axis), value)]
    unnamed x7 -> x0, waiting for transfers between devices: 46.5 us -> none
    select_n x30 -> x0, other arithmetic: 44.4 us -> none  [step(): jnp.where(position < mine, new, old)]
    pallas_call x0 -> x1, Pallas kernels: none -> 41.4 us  [shards(): pl.pallas_call(functools.partial(kernel, (n, tp, seqs, heads, length, dk,...]
    unnamed x1 -> x0, blocking collectives: 35.5 us -> none
    psum x1 -> x0, blocking collectives: 31.2 us -> none  [shards(): rate_sums = lax.psum(local_sums, 'sp')]
    dot_general x23 -> x0, matrix products: 29.3 us -> none  [the longest x1 2.18 us: input_rows(): jnp.einsum('blhk,dhk->bld', piece, key_weight, preferred_element_type=jnp...]
    mul x63 -> x0, local copies, waits for them, and re-layouts: 23.6 us -> none  [the longest x30 9.93 us: link_states(): later[0] * earlier[1] + later[1]]
  transfers between devices with their start and end apart: 6 -> 0, of which waited for: 6 -> 0; matrix products, arithmetic and copies ran while one was open for 20% -> 0% of each run, Pallas kernels for 0% -> 0%
where the time goes in v1:
time: 50.1 us; the launch traced here: 49.9 us
  Pallas kernels  41.4 us (83%)
  local copies, waits for them, and re-layouts  5.82 us (12%)
  other arithmetic  1.9 us (4%)
  between operations  0.74 us (1%)
    pallas_call x1, Pallas kernels, shards(): pl.pallas_call(functools.partial(kernel, (n, tp, seqs, heads, length, dk,...  41.4 us
    unnamed x14, local copies, waits for them, and re-layouts  3.05 us

profile of v1, /device:TPU:0, one launch (start us, length us, event | category | flops | bytes accessed | tf_op | source)
XLA Modules:
  0.0 49.9 jit_solution(15279313238213146149)
XLA Ops:
  0.6 0.0 copy-start.1
  0.6 0.0 copy-start.2
  0.7 0.0 copy-start.3
  0.7 0.8 %fusion.1.rates = f32[2,2]{1,0:T(2,128)S(1)} fusion(f32[1,2]{1,0:T(1,128)} %bitcast.23, f32[1,2]{1,0:T(1,128)} %bitcast.25), kind=kLoop, calls=%fused_computation.5 | loop fusion | flops 40 | bytes 32 | tf_op jit(solution)/shard_map/div | solution.py:276
  1.4 1.1 %copy.17 = bf16[128,8,2,128]{3,1,2,0:T(8,128)(2,1)S(1)} copy(bf16[128,8,2,128]{3,2,1,0:T(2,128)(2,1)} %bitcast.22) | data formatting | bytes 1048576
  2.6 0.0 copy-done.1
  2.6 0.0 copy-done.2
  2.6 0.0 copy-done.3
  2.6 0.6 %maximum_bitcast_fusion = bf16[2,2,128,640]{3,1,2,0:T(2,128)(2,1)S(1)} fusion(bf16[2,128,2,256]{3,2,1,0:T(2,128)(2,1)S(1)} %copy-done.1, bf16[2,128,2,256]{3,2,1,0:T(2,128)(2,1)S(1)} %copy-done.2, bf16[2,128,2,128]{3,2,1,0:T(2,128)(2,1)S(1)} %copy-done.3), kind=kLoop, calls=%fused_computation | loop fusion | flops 1966080 | bytes 1310720 | tf_op jit(solution)/shard_map/transpose | solution.py:278
  3.2 0.0 copy-start
  3.2 0.1 copy.12
  3.2 1.0 %copy-done = bf16[2,128,1024]{2,1,0:T(8,128)(2,1)S(1)} copy-done((bf16[2,128,1024]{2,1,0:T(8,128)(2,1)S(1)}, bf16[2,128,1024]{2,1,0:T(8,128)(2,1)}, u32[]{:S(2)}) %copy-start) | copy-done | bytes 524312
  4.2 41.4 %shard_map.110 = (bf16[4,128,384]{2,1,0:T(8,128)(2,1)S(1)}, bf16[128,1024]{1,0:T(8,128)(2,1)S(1)}, f32[64,256]{1,0:T(8,128)S(1)}, f32[8,128]{1,0:T(8,128)S(1)}) custom-call(f32[2,2]{1,0:T(2,128)S(1)} %fusion.1.rates, bf16[4,128,640]{2,1,0:T(8,128)(2,1)S(1)} %bitcast.15, bf16[256,1024]{1,0:T(8,128)(2,1)S(1)} %bitcast.17, bf16[1024,256]{1,0:T(8,128)(2,1)S(1)} %bitcast.16), custom_call_target="tpu_custom_call" | custom-call | tf_op jit(solution)/shard_map/pallas_call | solution.py:284
  45.6 0.0 copy-start.4
  45.6 0.0 copy-start.5
  45.6 0.4 copy.18
  46.0 0.2 copy-done.4
  46.3 0.0 copy-done.5
  46.3 0.6 %multiply_multiply_fusion = f32[2,2]{1,0:T(2,128)} fusion(f32[8,128]{1,0:T(8,128)S(1)} %get-tuple-element.12, f32[1,2]{1,0:T(1,128)S(1)} %bitcast.24, f32[1,2]{1,0:T(1,128)S(1)} %bitcast.26), kind=kLoop, calls=%fused_computation.7 | loop fusion | flops 20 | bytes 48 | tf_op jit(solution)/shard_map/mul | solution.py:332
  46.9 0.7 %reshape.33 = f32[64,2,128]{2,1,0:T(2,128)} reshape(f32[64,256]{1,0:T(8,128)S(1)} %get-tuple-element.11) | data formatting | bytes 131072 | tf_op jit(solution)/shard_map/reshape | solution.py:331
  47.5 0.7 %slice.12 = bf16[2,128,2,128]{3,2,1,0:T(2,128)(2,1)} slice(bf16[2,128,2,384]{3,2,1,0:T(2,128)(2,1)S(1)} %bitcast.20), slice={[0:2], [0:128], [0:2], [0:128]} | slice | bytes 262144 | tf_op jit(solution)/shard_map/slice | solution.py:328
  48.3 0.9 %slice.13 = bf16[2,128,2,256]{3,2,1,0:T(2,128)(2,1)} slice(bf16[2,128,2,384]{3,2,1,0:T(2,128)(2,1)S(1)} %bitcast.21), slice={[0:2], [0:128], [0:2], [128:384]} | slice | bytes 524288 | tf_op jit(solution)/shard_map/slice | solution.py:329
  49.2 0.7 %copy.20 = bf16[1,128,1024]{2,1,0:T(8,128)(2,1)} copy(bf16[1,128,1024]{2,1,0:T(8,128)(2,1)S(1)} %bitcast.19) | data formatting | bytes 524288
Async XLA Ops:
  0.6 1.9 %copy-start.1 = (bf16[2,128,2,256]{3,2,1,0:T(2,128)(2,1)S(1)}, bf16[2,128,2,256]{3,2,1,0:T(2,128)(2,1)}, u32[]{:S(2)}) copy-start(bf16[2,128,2,256]{3,2,1,0:T(2,128)(2,1)} %param.10) | copy-start | bytes 786436
  0.6 1.9 %copy-start.2 = (bf16[2,128,2,256]{3,2,1,0:T(2,128)(2,1)S(1)}, bf16[2,128,2,256]{3,2,1,0:T(2,128)(2,1)}, u32[]{:S(2)}) copy-start(bf16[2,128,2,256]{3,2,1,0:T(2,128)(2,1)} %param.9) | copy-start | bytes 786436
  0.7 1.9 %copy-start.3 = (bf16[2,128,2,128]{3,2,1,0:T(2,128)(2,1)S(1)}, bf16[2,128,2,128]{3,2,1,0:T(2,128)(2,1)}, u32[]{:S(2)}) copy-start(bf16[2,128,2,128]{3,2,1,0:T(2,128)(2,1)} %param.8) | copy-start | bytes 393220
  3.2 1.0 %copy-start = (bf16[2,128,1024]{2,1,0:T(8,128)(2,1)S(1)}, bf16[2,128,1024]{2,1,0:T(8,128)(2,1)}, u32[]{:S(2)}) copy-start(bf16[2,128,1024]{2,1,0:T(8,128)(2,1)} %param.7) | copy-start | bytes 1572868
  45.6 0.7 %copy-start.4 = (f32[2]{0:T(128)S(1)}, f32[2]{0:T(128)}, u32[]{:S(2)}) copy-start(f32[2]{0:T(128)} %param.13) | copy-start | bytes 28
  45.6 0.7 %copy-start.5 = (f32[2]{0:T(128)S(1)}, f32[2]{0:T(128)}, u32[]{:S(2)}) copy-start(f32[2]{0:T(128)} %param.12) | copy-start | bytes 28

commit v2 on v1

--- a/solution.py
+++ b/solution.py
@@ -21,12 +21,12 @@
 
 def kernel(
     cfg,
-    rates, pack, x, w,
-    gqv_out, ig_out, wg_out, dec_out,
-    tok, ktok, kown, local, arrive, leave,
+    ahead, behind, pack, x, w,
+    q_out, v_out, ig_out, wg_out, dec_out,
+    xt, mask, gm, tok, ktok, kown, local, arrive, leave,
     kgs, kgr, gqs, gqr, dbuf, dpair, dsum, dland,
     wb, wpair, wsum, wland, isend, iland,
-    tok_s, tok_r, k_s, k_r, ch_s, ch_r, kg_s, kg_r, gq_s, gq_r,
+    tok_s, tok_r, v_s, v_r, k_s, k_r, ch_s, ch_r, kg_s, kg_r, gq_s, gq_r,
     tp_s, tp_r, pr_s, pr_r, w_s, w_r, d_s, d_r,
 ):
     n, tp, seqs, heads, length, dk, dv, scale = cfg
@@ -69,12 +69,20 @@
         greeted += 1
     pl.semaphore_wait(barrier, greeted)
 
-    tok_copies, k_copies = [], []
-    for o in range(1, pairs):
-        to = (member + o) % pairs
-        copy = remote(pack.at[to], tok.at[member], tok_s.at[o], tok_r.at[o], {"sp": base + to})
+    early = dk + dv
+    tok_copies, v_copies, k_copies = [], [], []
+    for o in range(1, pairs):
+        to = (member + o) % pairs
+        copy = remote(pack.at[to, :, pl.ds(0, early)], tok.at[member, :, pl.ds(0, early)],
+                      tok_s.at[o], tok_r.at[o], {"sp": base + to})
         copy.start()
         tok_copies.append(copy)
+    for o in range(1, pairs):
+        to = (member + o) % pairs
+        copy = remote(pack.at[to, :, pl.ds(early, dv)], tok.at[member, :, pl.ds(early, dv)],
+                      v_s.at[o], v_r.at[o], {"sp": base + to})
+        copy.start()
+        v_copies.append(copy)
     key_raw = mm(x[...], w[...], NN).astype(BF16)
     for b in range(seqs):
         for h in range(heads):
@@ -87,87 +95,91 @@
     tok[member] = pack[member]
     ktok[member] = kown[member]
 
-    rate_a = rates[0, head]
-    rate_b = rates[1, head]
+    def rate_and_slope(ref):
+        raw = jnp.full((1, 1), ref[head], F32)
+        rate = jnp.minimum(raw, 0.0) - jnp.log(1.0 + jnp.exp(-jnp.abs(raw)))
+        return rate / (length * n), 1.0 / ((1.0 + jnp.exp(raw)) * (length * n))
+
+    rate_a, slope_a = rate_and_slope(ahead)
+    rate_b, slope_b = rate_and_slope(behind)
     off = lax.broadcasted_iota(jnp.int32, (chunk, 1), 0).astype(F32)
     keep_a = jnp.exp((chunk - 1.0 - off) * rate_a)
     keep_b = jnp.exp(off * rate_b)
     reach_a = jnp.exp((off + 1.0) * rate_a)
     reach_b = jnp.exp((chunk - off) * rate_b)
-    one = jnp.full((1, dv), float(chunk), F32)
-    spans = (jnp.exp(one * rate_a), jnp.exp(one * rate_b))
+    span_a = jnp.exp(chunk * rate_a)
+    span_b = jnp.exp(chunk * rate_b)
+    dist = (lax.broadcasted_iota(jnp.int32, (chunk, chunk), 0)
+            - lax.broadcasted_iota(jnp.int32, (chunk, chunk), 1)).astype(F32)
+    decay = jnp.exp(jnp.abs(dist) * jnp.where(dist >= 0, rate_a, rate_b))
+    mask[...] = jnp.where(dist == 0, 2.0, decay)
+    xt[...] = x[...].T
+
+    low = group < (groups + 1) // 2
+    piece = dk // 2
+
+    def chain(j, pull, finish=False):
+        way = jnp.where(low, j, 1 - j)
+        kind = 1 - way if pull else way
+        span = jnp.where(kind == 0, span_a, span_b)
+        has_in = jnp.where(way == 0, group > 0, group < groups - 1)
+        has_out = jnp.where(way == 0, group < groups - 1, group > 0)
+        nxt = jnp.clip(group + 1 - 2 * way, 0, groups - 1) * pairs + member
+        for c in range(2):
+            rows = pl.ds(c * piece, piece)
+            copy = remote(leave.at[way, kind, rows], arrive.at[way, kind, rows],
+                          ch_s.at[way, kind, c], ch_r.at[way, kind, c], {"sp": nxt})
+            if finish:
+                @pl.when(has_out)
+                def _():
+                    copy.wait_send()
+                continue
+
+            @pl.when(has_in)
+            def _():
+                copy.wait_recv()
+
+            @pl.when(jnp.logical_not(has_in))
+            def _():
+                arrive[way, kind, rows] = jnp.zeros((piece, dv), BF16)
+
+            @pl.when(has_out)
+            def _():
+                leave[way, kind, rows] = (
+                    span * arrive[way, kind, rows].astype(F32) + local[way, kind, rows]
+                ).astype(BF16)
+                copy.start()
 
     for copy in tok_copies:
         copy.wait_recv()
     q = tok[:, :, :dk].reshape(chunk, dk)
-    v = tok[:, :, dk:dk + dv].reshape(chunk, dv)
-    do = tok[:, :, dk + dv:].reshape(chunk, dv)
+    do = tok[:, :, dk:early].reshape(chunk, dv)
     qf = q.astype(F32)
     local[0, 1] = mm((qf * reach_b).astype(BF16), do, TN)
     local[1, 0] = mm((qf * reach_a).astype(BF16), do, TN)
+    chain(0, True)
+    for copy in v_copies:
+        copy.wait_recv()
+    v = tok[:, :, early:].reshape(chunk, dv)
+    gm[...] = mm(do, v, NT) * mask[...]
     for copy in k_copies:
         copy.wait_recv()
     k = ktok[...].reshape(chunk, dk)
     kf = k.astype(F32)
     local[0, 0] = mm((kf * keep_a).astype(BF16), v, TN)
     local[1, 1] = mm((kf * keep_b).astype(BF16), v, TN)
-
-    low = group < (groups + 1) // 2
-
-    def chain(j):
-        way = jnp.where(low, j, 1 - j)
-        has_in = jnp.where(way == 0, group > 0, group < groups - 1)
-        has_out = jnp.where(way == 0, group < groups - 1, group > 0)
-        nxt = jnp.clip(group + 1 - 2 * way, 0, groups - 1) * pairs + member
-        for kind in range(2):
-            copy = remote(leave.at[way, kind], arrive.at[way, kind], ch_s.at[way, kind],
-                          ch_r.at[way, kind], {"sp": nxt})
-
-            @pl.when(has_in)
-            def _():
-                copy.wait_recv()
-
-            @pl.when(jnp.logical_not(has_in))
-            def _():
-                arrive[way, kind] = jnp.zeros(arrive.shape[2:], BF16)
-
-            @pl.when(has_out)
-            def _():
-                leave[way, kind] = (
-                    spans[kind] * arrive[way, kind].astype(F32) + local[way, kind]
-                ).astype(BF16)
-                copy.start()
-
-    def chain_end(j):
-        way = jnp.where(low, j, 1 - j)
-        has_out = jnp.where(way == 0, group < groups - 1, group > 0)
-        nxt = jnp.clip(group + 1 - 2 * way, 0, groups - 1) * pairs + member
-        for kind in range(2):
-            copy = remote(leave.at[way, kind], arrive.at[way, kind], ch_s.at[way, kind],
-                          ch_r.at[way, kind], {"sp": nxt})
-
-            @pl.when(has_out)
-            def _():
-                copy.wait_send()
-
-    chain(0)
-    scores = mm(q, k, NT) * scale
-    grads = mm(do, v, NT)
-    dist = (lax.broadcasted_iota(jnp.int32, (chunk, chunk), 0)
-            - lax.broadcasted_iota(jnp.int32, (chunk, chunk), 1)).astype(F32)
-    gap = jnp.abs(dist)
-    decay = jnp.exp(gap * jnp.where(dist >= 0, rate_a, rate_b))
-    mask = jnp.where(dist == 0, 2.0, decay)
-    gm = grads * mask
-    weighted = gm * scores * gap
-    in_a = jnp.sum(jnp.where(dist > 0, weighted, 0.0))
-    in_b = jnp.sum(jnp.where(dist < 0, weighted, 0.0))
-    gm = gm.astype(BF16)
-    sm = (scores * mask).astype(BF16)
-    grad_q = mm(gm, k, NN)
-    grad_k = mm(gm, q, TN)
+    chain(0, False)
+    chain(1, True)
+    sm = mm(q, k, NT) * scale
+    weighted = gm[...] * sm
+    in_a = jnp.sum(weighted * jnp.maximum(dist, 0.0))
+    in_b = jnp.sum(weighted * jnp.maximum(-dist, 0.0))
+    sm = (sm * mask[...]).astype(BF16)
+    gmb = gm[...].astype(BF16)
+    grad_q = mm(gmb, k, NN)
+    grad_k = mm(gmb, q, TN)
     grad_v = mm(sm, do, TN)
-    chain(1)
+    chain(1, False)
 
     ka = keep_a * mm(v, arrive[1, 0], NT)
     kb = keep_b * mm(v, arrive[0, 1], NT)
@@ -192,8 +204,8 @@
         gq_copies.append(copy)
     gqr[member] = gqs[member]
     pos = off + ((group * chunk).astype(F32) - 0.5 * (chunk * groups))
-    sum_a = in_a + scale * jnp.sum(pos * (qf * qa - kf * ka))
-    sum_b = in_b + scale * jnp.sum(pos * (kf * kb - qf * qb))
+    sum_a = slope_a * (in_a + scale * jnp.sum(pos * (qf * qa - kf * ka)))
+    sum_b = slope_b * (in_b + scale * jnp.sum(pos * (kf * kb - qf * qb)))
     row = lax.broadcasted_iota(jnp.int32, dbuf.shape, 0)
     lane = lax.broadcasted_iota(jnp.int32, dbuf.shape, 1)
     dbuf[...] = jnp.where(lane == head, jnp.where(row == 0, sum_a, jnp.where(row == 1, sum_b, 0.0)), 0.0)
@@ -217,7 +229,7 @@
         copy.start()
         tp_copies.append(copy)
     kg_all = jnp.concatenate([seq_rows(b) for b in range(seqs)], axis=0)
-    wp = mm(x[...], kg_all, TN).astype(BF16).reshape(half, 2, -1, heads * dk)
+    wp = mm(xt[...], kg_all, NN).astype(BF16).reshape(half, 2, -1, heads * dk)
     wb[0] = wp[:, 0]
     wb[1] = wp[:, 1]
     w_pair = remote(wb.at[1 - parity], wpair, pr_s.at[0], pr_r.at[0], {"sp": partner})
@@ -241,7 +253,8 @@
         w_copies.append(copy)
     for copy in gq_copies:
         copy.wait_recv()
-    gqv_out[...] = gqr[...]
+    q_out[...] = gqr[:, :, :dk]
+    v_out[...] = gqr[:, :, dk:]
     for copy in tp_copies:
         copy.wait_recv()
     for s in range(own_seqs):
@@ -259,9 +272,10 @@
         copy.wait_recv()
         total = total + wland[o].astype(F32)
     wg_out[...] = total
-    chain_end(0)
-    chain_end(1)
-    for copy in (tok_copies + k_copies + kg_copies + gq_copies + tp_copies + w_copies + d_copies
+    for j in range(2):
+        chain(j, True, True)
+        chain(j, False, True)
+    for copy in (tok_copies + v_copies + k_copies + kg_copies + gq_copies + tp_copies + w_copies + d_copies
                  + [d_pair, w_pair]):
         copy.wait_send()
 
@@ -272,26 +286,30 @@
     pairs = seqs * heads
     all_tokens = length * n
     scale = 1.0 / math.sqrt(width * dk * all_tokens)
-    decays = jnp.stack([decay_ahead, decay_behind])
-    rates = jax.nn.log_sigmoid(decays) / all_tokens
-    pack = jnp.concatenate([queries, values, out_grad], axis=3)
+    pack = jnp.concatenate([queries, out_grad, values], axis=3)
     pack = pack.transpose(0, 2, 1, 3).reshape(pairs, length, dk + 2 * dv)
     x = inputs.reshape(seqs * length, width)
     w = key_weight.reshape(width, heads * dk)
     half, rows, own = n // 2, width // n, seqs // tp
     vm = pl.BlockSpec(memory_space=pltpu.VMEM)
+    sm = pl.BlockSpec(memory_space=pltpu.SMEM)
+    chunk = pairs * length
     dma = pltpu.SemaphoreType.DMA
-    gqv, ig, wg, dec = pl.pallas_call(
+    gq, gv, ig, wg, dec = pl.pallas_call(
         functools.partial(kernel, (n, tp, seqs, heads, length, dk, dv, scale)),
         out_shape=(
-            jax.ShapeDtypeStruct((pairs, length, dk + dv), BF16),
+            jax.ShapeDtypeStruct((pairs, length, dk), BF16),
+            jax.ShapeDtypeStruct((pairs, length, dv), BF16),
             jax.ShapeDtypeStruct((own * length, width), BF16),
             jax.ShapeDtypeStruct((rows, heads * dk), F32),
             jax.ShapeDtypeStruct((8, 128), F32),
         ),
-        in_specs=[pl.BlockSpec(memory_space=pltpu.SMEM), vm, vm, vm],
-        out_specs=(vm, vm, vm, vm),
+        in_specs=[sm, sm, vm, vm, vm],
+        out_specs=(vm, vm, vm, vm, vm),
         scratch_shapes=[
+            pltpu.VMEM((width, seqs * length), BF16),
+            pltpu.VMEM((chunk, chunk), F32),
+            pltpu.VMEM((chunk, chunk), F32),
             pltpu.VMEM((pairs, length, dk + 2 * dv), BF16),
             pltpu.VMEM((pairs, length, dk), BF16),
             pltpu.VMEM((pairs, length, dk), BF16),
@@ -313,7 +331,8 @@
             pltpu.VMEM((tp - 1, own * length, width), BF16),
             pltpu.VMEM((tp - 1, own * length, width), BF16),
             dma((pairs,)), dma((pairs,)), dma((pairs,)), dma((pairs,)),
-            dma((2, 2)), dma((2, 2)),
+            dma((pairs,)), dma((pairs,)),
+            dma((2, 2, 2)), dma((2, 2, 2)),
             dma((pairs,)), dma((pairs,)), dma((pairs,)), dma((pairs,)),
             dma((tp - 1,)), dma((tp - 1,)), dma((2,)), dma((2,)),
             dma((half - 1,)), dma((half - 1,)), dma((half - 1,)), dma((half - 1,)),
@@ -321,15 +340,17 @@
         compiler_params=pltpu.CompilerParams(
             collective_id=0, has_side_effects=True, vmem_limit_bytes=50 * 1024 * 1024
         ),
-    )(rates, pack, x, w)
-    gqv = gqv.reshape(seqs, heads, length, dk + dv).transpose(0, 2, 1, 3)
-    slopes = jax.nn.sigmoid(-decays) / all_tokens
+    )(decay_ahead, decay_behind, pack, x, w)
+
+    def tokens_first(grad):
+        return grad.reshape(seqs, heads, length, -1).transpose(0, 2, 1, 3)
+
     return (
-        gqv[..., :dk],
-        gqv[..., dk:],
+        tokens_first(gq),
+        tokens_first(gv),
         ig.reshape(own, length, width),
         wg.reshape(rows, heads, dk),
-        dec[:2, :heads] * slopes,
+        dec[:2, :heads],
     )
 
 

time: 50.1 us -> 46.5 us (0.928)
  Pallas kernels: 41.4 us -> 39.2 us
  other arithmetic: 1.9 us -> 0.57 us
    pallas_call x1, Pallas kernels: 41.4 us -> 39.2 us  [shards(): pl.pallas_call(functools.partial(kernel, (n, tp, seqs, heads, length, dk,...]
    reshape x1 -> x2, local copies, waits for them, and re-layouts: 0.41 us -> 1.76 us  [tokens_first(): return grad.reshape(seqs, heads, length, -1).transpose(0, 2, 1, 3)]
    slice x2 -> x1, local copies, waits for them, and re-layouts: 1.63 us -> 0.56 us  [shards(): dec[:2, :heads]]
    div x1 -> x0, other arithmetic: 0.75 us -> none  [shards(): rates = jax.nn.log_sigmoid(decays) / all_tokens]
    mul x1 -> x0, other arithmetic: 0.58 us -> none  [shards(): dec[:2, :heads] * slopes]
where the time goes in v2:
time: 46.5 us; the launch traced here: 46.4 us
  Pallas kernels  39.2 us (84%)
  local copies, waits for them, and re-layouts  5.91 us (13%)
  between operations  0.73 us (2%)
  other arithmetic  0.57 us (1%)
    pallas_call x1, Pallas kernels, shards(): pl.pallas_call(functools.partial(kernel, (n, tp, seqs, heads, length, dk,...  39.2 us
    unnamed x14, local copies, waits for them, and re-layouts  2.84 us
    reshape x2, local copies, waits for them, and re-layouts, tokens_first(): return grad.reshape(seqs, heads, length, -1).transpose(0, 2, 1, 3)  1.76 us

profile of v2, /device:TPU:0, one launch (start us, length us, event | category | flops | bytes accessed | tf_op | source)
XLA Modules:
  0.0 46.4 jit_solution(12044133478406470064)
XLA Ops:
  0.6 0.0 copy-start.4
  0.6 0.0 copy-start.3
  0.7 0.0 copy-start.5
  0.7 1.2 %copy.19 = bf16[128,8,2,128]{3,1,2,0:T(8,128)(2,1)S(1)} copy(bf16[128,8,2,128]{3,2,1,0:T(2,128)(2,1)} %bitcast.23) | data formatting | bytes 1048576
  1.9 0.0 copy-done.4
  1.9 0.0 copy-done.3
  1.9 0.0 copy-done.5
  1.9 0.6 %maximum_bitcast_fusion = bf16[2,2,128,640]{3,1,2,0:T(2,128)(2,1)S(1)} fusion(bf16[2,128,2,256]{3,2,1,0:T(2,128)(2,1)S(1)} %copy-done.3, bf16[2,128,2,256]{3,2,1,0:T(2,128)(2,1)S(1)} %copy-done.4, bf16[2,128,2,128]{3,2,1,0:T(2,128)(2,1)S(1)} %copy-done.5), kind=kLoop, calls=%fused_computation | loop fusion | flops 1966080 | bytes 1310720 | tf_op jit(solution)/shard_map/transpose | solution.py:290
  2.5 0.0 copy-start
  2.5 0.0 copy-start.1
  2.5 0.0 copy-start.2
  2.5 0.1 copy.12
  2.6 0.9 %copy-done = bf16[2,128,1024]{2,1,0:T(8,128)(2,1)S(1)} copy-done((bf16[2,128,1024]{2,1,0:T(8,128)(2,1)S(1)}, bf16[2,128,1024]{2,1,0:T(8,128)(2,1)}, u32[]{:S(2)}) %copy-start) | copy-done | bytes 524312
  3.5 0.0 copy-done.1
  3.5 0.0 copy-done.2
  3.5 39.2 %shard_map.110 = (bf16[4,128,128]{2,1,0:T(8,128)(2,1)S(1)}, bf16[4,128,256]{2,1,0:T(8,128)(2,1)S(1)}, bf16[128,1024]{1,0:T(8,128)(2,1)S(1)}, f32[64,256]{1,0:T(8,128)S(1)}, f32[8,128]{1,0:T(8,128)S(1)}) custom-call(f32[2]{0:T(128)S(1)} %copy-done.1, f32[2]{0:T(128)S(1)} %copy-done.2, bf16[4,128,640]{2,1,0:T(8,128)(2,1)S(1)} %bitcast.17, ...), custom_call_target="tpu_custom_call" | custom-call | tf_op jit(solution)/shard_map/pallas_call | solution.py:298
  42.7 0.8 %copy.21 = bf16[2,2,128,128]{3,1,2,0:T(2,128)(2,1)} copy(bf16[2,2,128,128]{3,2,1,0:T(8,128)(2,1)S(1)} %bitcast.22) | data formatting | bytes 262144 | tf_op jit(solution)/shard_map/reshape | solution.py:346
  43.5 1.0 %copy.20 = bf16[2,2,128,256]{3,1,2,0:T(2,128)(2,1)} copy(bf16[2,2,128,256]{3,2,1,0:T(8,128)(2,1)S(1)} %bitcast.21) | data formatting | bytes 524288 | tf_op jit(solution)/shard_map/reshape | solution.py:346
  44.5 0.6 %slice.3 = f32[2,2]{1,0:T(2,128)} slice(f32[8,128]{1,0:T(8,128)S(1)} %get-tuple-element.14), slice={[0:2], [0:2]} | slice | bytes 32 | tf_op jit(solution)/shard_map/slice | solution.py:353
  45.0 0.7 %reshape.37 = f32[64,2,128]{2,1,0:T(2,128)} reshape(f32[64,256]{1,0:T(8,128)S(1)} %get-tuple-element.13) | data formatting | bytes 131072 | tf_op jit(solution)/shard_map/reshape | solution.py:352
  45.7 0.7 %copy.23 = bf16[1,128,1024]{2,1,0:T(8,128)(2,1)} copy(bf16[1,128,1024]{2,1,0:T(8,128)(2,1)S(1)} %bitcast.20) | data formatting | bytes 524288
Async XLA Ops:
  0.6 1.2 %copy-start.4 = (bf16[2,128,2,256]{3,2,1,0:T(2,128)(2,1)S(1)}, bf16[2,128,2,256]{3,2,1,0:T(2,128)(2,1)}, u32[]{:S(2)}) copy-start(bf16[2,128,2,256]{3,2,1,0:T(2,128)(2,1)} %param.10) | copy-start | bytes 786436
  0.6 1.2 %copy-start.3 = (bf16[2,128,2,256]{3,2,1,0:T(2,128)(2,1)S(1)}, bf16[2,128,2,256]{3,2,1,0:T(2,128)(2,1)}, u32[]{:S(2)}) copy-start(bf16[2,128,2,256]{3,2,1,0:T(2,128)(2,1)} %param.9) | copy-start | bytes 786436
  0.7 1.2 %copy-start.5 = (bf16[2,128,2,128]{3,2,1,0:T(2,128)(2,1)S(1)}, bf16[2,128,2,128]{3,2,1,0:T(2,128)(2,1)}, u32[]{:S(2)}) copy-start(bf16[2,128,2,128]{3,2,1,0:T(2,128)(2,1)} %param.8) | copy-start | bytes 393220
  2.5 1.0 %copy-start = (bf16[2,128,1024]{2,1,0:T(8,128)(2,1)S(1)}, bf16[2,128,1024]{2,1,0:T(8,128)(2,1)}, u32[]{:S(2)}) copy-start(bf16[2,128,1024]{2,1,0:T(8,128)(2,1)} %param.7) | copy-start | bytes 1572868
  2.5 1.0 %copy-start.1 = (f32[2]{0:T(128)S(1)}, f32[2]{0:T(128)}, u32[]{:S(2)}) copy-start(f32[2]{0:T(128)} %ahead.1) | copy-start | bytes 28
  2.5 1.0 %copy-start.2 = (f32[2]{0:T(128)S(1)}, f32[2]{0:T(128)}, u32[]{:S(2)}) copy-start(f32[2]{0:T(128)} %behind.1) | copy-start | bytes 28
